TPU v7x, 32 devices: a whole 2x2x4 slice. The times are simulated.
32 devices in a mesh: sp: 16 (over z, y, core), dp: 2 (over x).
Axes of the slice: x: 2, y: 2, z: 4, core: 2. Of those that a mesh axis runs over, the one named last changes fastest.
Arguments:
- signal: bfloat16 [2, 2048, 1024], P('dp', 'sp'), may hold values from -6 to 6
- pace: float32 [2, 16], P('dp'), may hold values from 0.5 to 2
- log_step: float32 [64], P('sp'), may hold values from -5.52 to -4.42
- a_real: float32 [64, 64], P('sp'), may hold values from -4 to -0.002, as said below
- a_imag: float32 [64, 64], P('sp'), may hold values from 0.5 to 201.06177
- in_map: float32 [64, 2, 64, 16], P('sp'), may hold values from -3 to 3
- out_map: float32 [64, 2, 16, 64], P('sp'), may hold values from -0.5 to 0.5
- skip: float32 [1024], P('sp'), may hold values from -1 to 1
- init_state: float32 [2, 2, 64, 64], P('dp', None, 'sp'), may hold values from -5 to 5
- w_glu: bfloat16 [1024, 1024], P('sp', 'dp'), may hold values from -0.1875 to 0.1875
- b_glu: float32 [1024], replicated, may hold values from -4 to 4
- g_mix: float32 [1024], replicated, may hold values from 0.1 to 1.9
- w_out: bfloat16 [1024, 4096], P('sp', 'dp'), may hold values from -0.1875 to 0.1875
Outputs:
- result: bfloat16 [2, 2048, 4096], P('dp', 'sp')
Inputs may be any that keep to these rules, and one draw needn't show every extreme that they name: `a_real`: negative entries; within a group all entries are of one order.
All inputs are finite; a program needn't handle non-finite values.
Results may differ from a plain program's by a relative error of at most 0.0075.
Values may be sent and summed in bfloat16 or wider, within the bound.
A program may use at most 64 MiB of HBM per device.

v0:
```python
import jax
import jax.numpy as jnp
from jax import lax
from jax.sharding import PartitionSpec as P


def combine(first, second):
    a1r, a1i, b1r, b1i = first
    a2r, a2i, b2r, b2i = second
    return (
        a2r * a1r - a2i * a1i,
        a2r * a1i + a2i * a1r,
        a2r * b1r - a2i * b1i + b2r,
        a2r * b1i + a2i * b1r + b2i,
    )


def mix_group(series, pace_row, log_rate, a_re, a_im, in_map, out_map, skip_row, init):
    blocks_count = pace_row.shape[0]
    length = series.shape[0]
    span = length // blocks_count
    states = a_re.shape[0]
    steps = (jnp.exp(log_rate) * pace_row)[:, None]
    decay = jnp.exp(a_re * steps)
    bar_re = decay * jnp.cos(a_im * steps)
    bar_im = decay * jnp.sin(a_im * steps)
    modulus = a_re * a_re + a_im * a_im
    coef_re = ((bar_re - 1.0) * a_re + bar_im * a_im) / modulus
    coef_im = (bar_im * a_re - (bar_re - 1.0) * a_im) / modulus
    drive_re = coef_re[..., None] * in_map[0] - coef_im[..., None] * in_map[1]
    drive_im = coef_re[..., None] * in_map[1] + coef_im[..., None] * in_map[0]
    drive = jnp.concatenate([drive_re, drive_im], axis=1).astype(jnp.bfloat16)
    blocks = series.reshape(blocks_count, span, series.shape[1])
    inject = jnp.einsum("kpc,ksc->kps", drive, blocks, preferred_element_type=jnp.float32)
    inner_re = inject[:, :states]
    inner_im = inject[:, states:]
    power_re = bar_re[..., None]
    power_im = bar_im[..., None]
    offset = 1
    while offset < span:
        moved_re = jnp.pad(inner_re[..., :-offset], ((0, 0), (0, 0), (offset, 0)))
        moved_im = jnp.pad(inner_im[..., :-offset], ((0, 0), (0, 0), (offset, 0)))
        inner_re, inner_im = (
            inner_re + power_re * moved_re - power_im * moved_im,
            inner_im + power_re * moved_im + power_im * moved_re,
        )
        power_re, power_im = (power_re * power_re - power_im * power_im, 2.0 * power_re * power_im)
        offset = offset * 2
    ends_re = (
        inner_re[:, :, -1].at[0].add(power_re[0, :, 0] * init[0] - power_im[0, :, 0] * init[1])
    )
    ends_im = (
        inner_im[:, :, -1].at[0].add(power_re[0, :, 0] * init[1] + power_im[0, :, 0] * init[0])
    )
    carried = lax.associative_scan(
        combine, (power_re[..., 0], power_im[..., 0], ends_re, ends_im), axis=0
    )
    before_re = jnp.concatenate([init[0][None], carried[2][:-1]], axis=0)[..., None]
    before_im = jnp.concatenate([init[1][None], carried[3][:-1]], axis=0)[..., None]
    places = (jnp.arange(span, dtype=jnp.float32) + 1.0)[None, None, :]
    scaled = steps[:, :, None] * places
    magnitude = jnp.exp(a_re[None, :, None] * scaled)
    angle = a_im[None, :, None] * scaled
    lift_re = magnitude * jnp.cos(angle)
    lift_im = magnitude * jnp.sin(angle)
    state_re = inner_re + lift_re * before_re - lift_im * before_im
    state_im = inner_im + lift_re * before_im + lift_im * before_re
    highest = lax.Precision.HIGHEST
    response = jnp.einsum("cp,kps->ksc", out_map[0], state_re, precision=highest) - jnp.einsum(
        "cp,kps->ksc", out_map[1], state_im, precision=highest
    )
    response = response.reshape(length, series.shape[1]) + skip_row * series.astype(jnp.float32)
    return jax.nn.gelu(response).astype(jnp.bfloat16)


def folder(left, piece):
    return jnp.dot(left, piece, preferred_element_type=jnp.float32)


def per_device(
    signal,
    pace,
    log_step,
    a_real,
    a_imag,
    in_map,
    out_map,
    skip,
    init_state,
    w_glu,
    b_glu,
    g_mix,
    w_out,
):
    local_seqs = signal.shape[0]
    tokens = signal.shape[1]
    width = signal.shape[2]
    groups = a_real.shape[0]
    channels = width // (groups * lax.axis_size("sp"))
    grouped = lax.all_to_all(signal, "sp", split_axis=2, concat_axis=1, tiled=True)
    length = grouped.shape[1]
    skips = skip.reshape(groups, channels)

    def per_sequence(inputs):
        sample, pace_row, init_row = inputs
        series = sample.reshape(length, groups, channels)
        outputs = jax.vmap(mix_group, in_axes=(1, None, 0, 0, 0, 0, 0, 0, 1), out_axes=1)(
            series, pace_row, log_step, a_real, a_imag, in_map, out_map, skips, init_row
        )
        return outputs.reshape(length, groups * channels)

    local_act = lax.map(per_sequence, (grouped, pace, init_state))
    activated = lax.all_to_all(local_act, "sp", split_axis=1, concat_axis=2, tiled=True)
    rows = activated.reshape(local_seqs * tokens, width)
    glu_cols, out_cols = (
        lax.all_gather(w_glu, "dp", axis=1, tiled=True),
        lax.all_gather(w_out, "dp", axis=1, tiled=True),
    )
    gate_pre = folder(rows, lax.all_gather(glu_cols, "sp", axis=0, tiled=True)) + b_glu
    gated = rows.astype(jnp.float32) * jax.nn.sigmoid(gate_pre)
    scale = lax.rsqrt(jnp.mean(gated * gated, axis=-1, keepdims=True) + 1e-06)
    mixed = (gated * scale * g_mix).astype(jnp.bfloat16)
    output = folder(mixed, lax.all_gather(out_cols, "sp", axis=0, tiled=True)).astype(jnp.bfloat16)
    return output.reshape(local_seqs, tokens, output.shape[1])


def solution(mesh):
    in_specs = (
        P("dp", "sp", None),
        P("dp", None),
        P("sp"),
        P("sp", None),
        P("sp", None),
        P("sp", None, None, None),
        P("sp", None, None, None),
        P("sp"),
        P("dp", None, "sp", None),
        P("sp", "dp"),
        P(),
        P(),
        P("sp", "dp"),
    )
    out_specs = P("dp", "sp", None)
    return jax.shard_map(
        per_device, mesh=mesh, in_specs=in_specs, out_specs=out_specs, check_vma=False
    )
```

profile of v0, /device:TPU:0, one launch (start us, length us, event | category | flops | bytes accessed | tf_op | source)
XLA Modules:
  0.0 147.8 jit_solution(5512769175658030008)
XLA Ops:
  6.5 7.8 %all_gather.12 = bf16[64,1024]{1,0:T(8,128)(2,1)} all-gather(bf16[64,512]{1,0:T(8,128)(2,1)} %param.26), channel_id=1, replica_groups=mesh['sp'=16,'dp'=2] {'dp'}, dimensions={1}, use_global_device_ids=true | all-gather | bytes 196608 | tf_op jit(solution)/shard_map/all_gather | solution.py:116
  14.4 8.4 %all_gather.14 = bf16[64,4096]{1,0:T(8,128)(2,1)} all-gather(bf16[64,2048]{1,0:T(8,128)(2,1)} %param.29), channel_id=1, replica_groups=mesh['sp'=16,'dp'=2] {'dp'}, dimensions={1}, use_global_device_ids=true | all-gather | bytes 786432 | tf_op jit(solution)/shard_map/all_gather | solution.py:117
  22.8 1.3 copy.90
  24.6 2.2 %reduce.14 = bf16[1024,128]{1,0:T(8,128)(2,1)S(1)} reduce(bf16[1024,1,128]{2,1,0:T(2,128)(2,1)S(1)} %bitcast.149, bf16[]{:T(256)} %broadcast.764), dimensions={1}, to_apply=%bitcast.92.reduce_sub_computation | reduce | bytes 524290
  26.8 0.8 reshape.452
  27.5 6.2 %all-to-all-start = ((bf16[16,2,4096]{2,1,0:T(2,128)(2,1)}), bf16[16,2,4096]{2,1,0:T(2,128)(2,1)S(1)}, u32[]{:S(2)}, u32[]{:S(2)}) async-start(bf16[16,2,4096]{2,1,0:T(2,128)(2,1)} %reshape.452), calls=%async_computation | async-start | bytes 524288 | tf_op jit(solution)/shard_map/all_to_all | solution.py:100
  35.7 8.1 %all-to-all-done = bf16[16,2,4096]{2,1,0:T(2,128)(2,1)S(1)} async-done(((bf16[16,2,4096]{2,1,0:T(2,128)(2,1)}), bf16[16,2,4096]{2,1,0:T(2,128)(2,1)S(1)}, u32[]{:S(2)}, u32[]{:S(2)}) %all-to-all-start) | async-done | bytes 262176 | tf_op jit(solution)/shard_map/all_to_all | solution.py:100
  44.4 1.4 fusion.48
  46.5 2.5 %fusion.4 = (f32[4,16,64,128]{3,2,1,0:T(8,128)S(1)}, f32[4,16,64,128]{3,2,1,0:T(8,128)S(1)}) fusion(f32[4,16,128,128]{3,2,1,0:T(8,128)S(1)} %fusion.48, f32[4,16,64,127]{3,2,1,0:T(8,128)S(1)} %get-tuple-element.102, f32[4,16,64,127]{3,2,1,0:T(8,128)S(1)} %get-tuple-element.101, f32[4,16,64]{2,1,0:T(8,128)S(1)} %get-tuple-element.151, ...), kind=kLoop, calls=%fused_computation.11 | loop fusion | flops 4194304 | bytes 12582912 | tf_op jit(solution)/shard_map/while/body/eval_jaxpr/vmap()/sub | solution.py:44
  49.0 2.5 %multiply_subtract_fusion.5 = (f32[4,16,64,128]{3,2,1,0:T(8,128)S(1)}, f32[4,16,64,128]{3,2,1,0:T(8,128)S(1)}) fusion(f32[4,16,64,128]{3,2,1,0:T(8,128)S(1)} %get-tuple-element.87, f32[4,16,64,126]{3,2,1,0:T(8,128)S(1)} %bitcast.135, f32[4,16,64,126]{3,2,1,0:T(8,128)S(1)} %bitcast.134, f32[4,16,64]{2,1,0:T(8,128)S(1)} %get-tuple-element.152, ...), kind=kLoop, calls=%fused_computation.34 | loop fusion | flops 4194304 | bytes 12550144 | tf_op jit(solution)/shard_map/while/body/eval_jaxpr/vmap()/sub | solution.py:44
  51.5 2.5 %multiply_subtract_fusion.4 = (f32[4,16,64,128]{3,2,1,0:T(8,128)S(1)}, f32[4,16,64,128]{3,2,1,0:T(8,128)S(1)}) fusion(f32[4,16,64,128]{3,2,1,0:T(8,128)S(1)} %get-tuple-element.99, f32[4,16,64,124]{3,2,1,0:T(8,128)S(1)} %bitcast.139, f32[4,16,64,124]{3,2,1,0:T(8,128)S(1)} %bitcast.138, f32[4,16,64]{2,1,0:T(8,128)S(1)} %get-tuple-element.148, ...), kind=kLoop, calls=%fused_computation.32 | loop fusion | flops 4194304 | bytes 12484608 | tf_op jit(solution)/shard_map/while/body/eval_jaxpr/vmap()/sub | solution.py:44
  54.1 2.5 %multiply_subtract_fusion.3 = (f32[4,16,64,128]{3,2,1,0:T(8,128)S(1)}, f32[4,16,64,128]{3,2,1,0:T(8,128)S(1)}) fusion(f32[4,16,64,128]{3,2,1,0:T(8,128)S(1)} %get-tuple-element.97, f32[4,16,64,120]{3,2,1,0:T(8,128)S(1)} %bitcast.141, f32[4,16,64,120]{3,2,1,0:T(8,128)S(1)} %bitcast.140, f32[4,16,64]{2,1,0:T(8,128)S(1)} %get-tuple-element.146, ...), kind=kLoop, calls=%fused_computation.30 | loop fusion | flops 4194304 | bytes 12353536 | tf_op jit(solution)/shard_map/while/body/eval_jaxpr/vmap()/sub | solution.py:44
  56.6 2.5 %multiply_subtract_fusion.2 = (f32[4,16,64,128]{3,2,1,0:T(8,128)S(1)}, f32[4,16,64,128]{3,2,1,0:T(8,128)S(1)}) fusion(f32[4,16,64,128]{3,2,1,0:T(8,128)S(1)} %get-tuple-element.95, f32[4,16,64,112]{3,2,1,0:T(8,128)S(1)} %bitcast.143, f32[4,16,64,112]{3,2,1,0:T(8,128)S(1)} %bitcast.142, f32[4,16,64]{2,1,0:T(8,128)S(1)} %get-tuple-element.144, ...), kind=kLoop, calls=%fused_computation.28 | loop fusion | flops 4194304 | bytes 12091392 | tf_op jit(solution)/shard_map/while/body/eval_jaxpr/vmap()/sub | solution.py:44
  59.1 2.5 %multiply_subtract_fusion.1 = (f32[4,16,64,128]{3,2,1,0:T(8,128)S(1)}, f32[4,16,64,128]{3,2,1,0:T(8,128)S(1)}) fusion(f32[4,16,64,128]{3,2,1,0:T(8,128)S(1)} %get-tuple-element.93, f32[4,16,64,96]{3,2,1,0:T(8,128)S(1)} %bitcast.145, f32[4,16,64,96]{3,2,1,0:T(8,128)S(1)} %bitcast.144, f32[4,16,64]{2,1,0:T(8,128)S(1)} %get-tuple-element.142, ...), kind=kLoop, calls=%fused_computation.26 | loop fusion | flops 4194304 | bytes 11567104 | tf_op jit(solution)/shard_map/while/body/eval_jaxpr/vmap()/sub | solution.py:44
  61.7 2.5 %multiply_subtract_fusion = (f32[4,16,64,128]{3,2,1,0:T(8,128)S(1)}, f32[4,16,64,128]{3,2,1,0:T(8,128)S(1)}) fusion(f32[4,16,64,128]{3,2,1,0:T(8,128)S(1)} %get-tuple-element.91, f32[4,16,64,64]{3,2,1,0:T(8,128)S(1)} %bitcast.137, f32[4,16,64,64]{3,2,1,0:T(8,128)S(1)} %bitcast.136, f32[4,16,64]{2,1,0:T(8,128)S(1)} %get-tuple-element.140, ...), kind=kLoop, calls=%fused_computation.24 | loop fusion | flops 4194304 | bytes 10518528 | tf_op jit(solution)/shard_map/while/body/eval_jaxpr/vmap()/sub | solution.py:44
  64.5 2.2 %slice_reduce_fusion = (f32[4,16,64]{2,1,0:T(8,128)S(1)}, f32[4,16,64]{2,1,0:T(8,128)S(1)}) fusion(f32[4,16,64,128]{3,2,1,0:T(8,128)S(1)} %get-tuple-element.90, f32[4,16,64,128]{3,2,1,0:T(8,128)S(1)} %get-tuple-element.89), kind=kLoop, calls=%fused_computation.6 | loop fusion | bytes 65536 | tf_op jit(solution)/shard_map/while/body/eval_jaxpr/vmap()/slice | solution.py:53
  68.6 11.0 %fusion.5 = f32[4,16,128,16]{2,3,1,0:T(8,128)S(1)} fusion(f32[4,16,64,128]{3,2,1,0:T(8,128)} %copy-done, f32[4,16,64]{2,1,0:T(8,128)S(1)} %pad_maximum_fusion.1, f32[4,16,64]{2,1,0:T(8,128)S(1)} %pad_maximum_fusion, f32[4,64]{1,0:T(4,128)S(1)} %copy-done.3, f32[4,16,128]{2,1,0:T(8,128)S(1)} %broadcast_multiply_fusion.6, f32[4,64]{1,0:T(4,128)S(1)} %copy-done.4, ...), kind=kOutput, calls=%fused_computation.12 | convolution fusion | flops 104857600 | bytes 2756608 | tf_op jit(solution)/shard_map/while/body/eval_jaxpr/vmap(cp,kps->ksc)/dot_general | solution.py:69
  79.6 9.9 %fusion.22 = f32[4,16,2,8,128]{4,3,2,1,0:T(8,128)S(1)} fusion(f32[4,16,128,16]{2,3,1,0:T(8,128)S(1)} %fusion.5, f32[4,16,64,128]{3,2,1,0:T(8,128)S(1)} %get-tuple-element.89, f32[4,16,64]{2,1,0:T(8,128)S(1)} %pad_maximum_fusion.1, f32[4,16,64]{2,1,0:T(8,128)S(1)} %pad_maximum_fusion, f32[4,64]{1,0:T(4,128)S(1)} %copy-done.3, ...), kind=kOutput, calls=%fused_computation.36 | convolution fusion | flops 104988672 | bytes 3280896 | tf_op jit(solution)/shard_map/while/body/eval_jaxpr/vmap(cp,kps->ksc)/dot_general | solution.py:69
  89.9 0.7 copy.127
  90.6 11.4 %reduce.15 = bf16[2048,64]{1,0:T(8,128)(2,1)S(1)} reduce(bf16[2048,1,64]{2,1,0:T(2,128)(2,1)S(1)} %bitcast.147, bf16[]{:T(256)} %broadcast.764), dimensions={1}, to_apply=%bitcast.94.reduce_sub_computation | reduce | bytes 524290
  102.5 20.1 %all_to_all.30 = bf16[16,2,4096]{2,1,0:T(2,128)(2,1)S(1)} all-to-all(bf16[16,2,4096]{2,1,0:T(2,128)(2,1)S(1)} %reshape.454), channel_id=1, replica_groups=mesh['sp'=16,'dp'=2] {'sp'}, dimensions={0} | all-to-all | bytes 524288 | tf_op jit(solution)/shard_map/all_to_all | solution.py:113
  124.2 2.2 %multiply_reduce_fusion = (f32[128]{0:T(128)S(1)}, f32[128,1024]{1,0:T(8,128)S(1)}) fusion(f32[1024]{0:T(1024)S(1)} %copy-done.9, bf16[128,1024]{0,1:T(8,128)(2,1)S(1)} %bitcast.153, bf16[1024,1024]{1,0:T(8,128)(2,1)} %all-gather.3.cloned.1.call-done, bf16[128,1024]{1,0:T(8,128)(2,1)S(1)} %copy.130), kind=kOutput, calls=%fused_computation.64 | convolution fusion | flops 269483904 | bytes 3150336 | tf_op jit(solution)/shard_map/dot_general | solution.py:77
  126.4 8.8 %all-gather.5.cloned.1.call-done = bf16[1024,4096]{1,0:T(8,128)(2,1)} async-done(((bf16[64,4096]{1,0:T(8,128)(2,1)}), bf16[1024,4096]{1,0:T(8,128)(2,1)}) %all-gather.5.cloned.1.call-update) | async-done | bytes 8388624 | tf_op jit(solution)/shard_map/all_gather | solution.py:123
  135.3 5.7 %fusion = bf16[1,128,4096]{2,1,0:T(8,128)(2,1)} fusion(bf16[1024,4096]{1,0:T(8,128)(2,1)} %all-gather.5.cloned.1.call-done, f32[128,1024]{1,0:T(8,128)S(1)} %get-tuple-element.161, f32[1024]{0:T(1024)S(1)} %copy-done.1, f32[128]{0:T(128)S(1)} %add_rsqrt_fusion), kind=kOutput, calls=%fused_computation.1 | convolution fusion | flops 1074659328 | bytes 9966080 | tf_op jit(solution)/shard_map/dot_general | solution.py:77
  (140 shorter events, 7.7 us)
Async XLA Ops:
  6.5 27.2 %copy-start.10 = (f32[4]{0:T(128)S(1)}, f32[4]{0:T(128)}, u32[]{:S(2)}) copy-start(f32[4]{0:T(128)} %param.19) | copy-start | bytes 52
  6.5 27.2 %copy-start.7 = (f32[1,16]{1,0:T(1,128)S(1)}, f32[1,16]{1,0:T(1,128)}, u32[]{:S(2)}) copy-start(f32[1,16]{1,0:T(1,128)} %param.18) | copy-start | bytes 196
  6.5 27.4 %copy-start.4 = (f32[4,64]{1,0:T(4,128)S(1)}, f32[4,64]{1,0:T(4,128)}, u32[]{:S(2)}) copy-start(f32[4,64]{1,0:T(4,128)} %param.20) | copy-start | bytes 3076
  6.5 117.6 %all-gather.3.cloned.1.call-start = ((), (), s32[]{:S(2)}) async-start(), calls=%async_computation.2 | async-start | bytes 2228224 | tf_op jit(solution)/shard_map/all_gather | solution.py:119
  14.3 19.7 %copy-start.3 = (f32[4,64]{1,0:T(4,128)S(1)}, f32[4,64]{1,0:T(4,128)}, u32[]{:S(2)}) copy-start(f32[4,64]{1,0:T(4,128)} %param.21) | copy-start | bytes 3076
  14.3 120.9 %all-gather.5.cloned.1.call-start = ((), (), s32[]{:S(2)}) async-start(), calls=%async_computation.3 | async-start | bytes 8912896 | tf_op jit(solution)/shard_map/all_gather | solution.py:123
  24.1 11.3 %copy-start.5 = (f32[1,2,4,64]{3,2,1,0:T(4,128)S(1)}, f32[1,2,4,64]{3,2,1,0:T(4,128)}, u32[]{:S(2)}) copy-start(f32[1,2,4,64]{3,2,1,0:T(4,128)} %param.25) | copy-start | bytes 6148
  24.6 10.9 %copy-start.6 = (f32[64]{0:T(128)S(1)}, f32[64]{0:T(128)}, u32[]{:S(2)}) copy-start(f32[64]{0:T(128)} %param.24) | copy-start | bytes 772
  24.6 11.0 %copy-start.2 = (f32[4,2,64,16]{2,3,1,0:T(8,128)S(1)}, f32[4,2,64,16]{2,3,1,0:T(8,128)}, u32[]{:S(2)}) copy-start(f32[4,2,64,16]{2,3,1,0:T(8,128)} %param.22) | copy-start | bytes 98308
  27.5 16.3 %all-to-all-start = ((bf16[16,2,4096]{2,1,0:T(2,128)(2,1)}), bf16[16,2,4096]{2,1,0:T(2,128)(2,1)S(1)}, u32[]{:S(2)}, u32[]{:S(2)}) async-start(bf16[16,2,4096]{2,1,0:T(2,128)(2,1)} %reshape.452), calls=%async_computation | async-start | bytes 524288 | tf_op jit(solution)/shard_map/all_to_all | solution.py:100
  64.2 2.6 %copy-start = (f32[4,16,64,128]{3,2,1,0:T(8,128)}, f32[4,16,64,128]{3,2,1,0:T(8,128)S(1)}, u32[]{:S(2)}) copy-start(f32[4,16,64,128]{3,2,1,0:T(8,128)S(1)} %get-tuple-element.90) | copy-start | bytes 6291460
  66.7 1.8 %copy-start.8 = (f32[4,2,16,64]{3,2,1,0:T(8,128)S(1)}, f32[4,2,16,64]{3,2,1,0:T(8,128)}, u32[]{:S(2)}) copy-start(f32[4,2,16,64]{3,2,1,0:T(8,128)} %param.23) | copy-start | bytes 98308
  122.6 1.6 %copy-start.9 = (f32[1024]{0:T(1024)S(1)}, f32[1024]{0:T(1024)}, u32[]{:S(2)}) copy-start(f32[1024]{0:T(1024)} %param.27) | copy-start | bytes 12292
  124.1 11.2 %copy-start.1 = (f32[1024]{0:T(1024)S(1)}, f32[1024]{0:T(1024)}, u32[]{:S(2)}) copy-start(f32[1024]{0:T(1024)} %param.28) | copy-start | bytes 12292
Sparse Core Ops, SparseCore 0:
  14.5 41.9 all-gather.2
  58.6 76.6 all-gather.4
where the time goes:
time: 148 us
  blocking collectives  36.3 us (25%)
  other arithmetic  33.4 us (23%)
  matrix products  30.3 us (20%)
  waiting for transfers between devices  17 us (11%)
  between operations  14.1 us (10%)
  local copies, waits for them, and re-layouts  10.5 us (7%)
  starting transfers between devices  6.23 us (4%)
    all_to_all x1, blocking collectives, per_device(): lax.all_to_all(local_act, 'sp', split_axis=1, concat_axis=2, tiled=True)  20.1 us
    sub x7, other arithmetic, mix_group(): inner_re + power_re * moved_re - power_im * moved_im  17.7 us
    unnamed x2, other arithmetic  13.6 us
    dot_general x1, matrix products, mix_group(): jnp.einsum('cp,kps->ksc', out_map[1], state_im, precision=highest)  11 us
    dot_general x1, matrix products, mix_group(): jnp.einsum('cp,kps->ksc', out_map[0], state_re, precision=highest)  9.95 us
    all_gather x1, waiting for transfers between devices, per_device(): lax.all_gather(out_cols, 'sp', axis=0, tiled=True)  8.84 us
    all_gather x1, blocking collectives, per_device(): lax.all_gather(w_out, 'dp', axis=1, tiled=True)  8.38 us
    all_to_all x1, waiting for transfers between devices, per_device(): lax.all_to_all(signal, 'sp', split_axis=2, concat_axis=1, tiled=True)  8.07 us
  transfers between devices with their start and end apart: 3, of which 2 were waited for; matrix products, arithmetic and copies ran while one was open for 46% of the time, Pallas kernels for 0%

commit v1 on v0

--- a/solution.py
+++ b/solution.py
@@ -112,10 +112,11 @@
     local_act = lax.map(per_sequence, (grouped, pace, init_state))
     activated = lax.all_to_all(local_act, "sp", split_axis=1, concat_axis=2, tiled=True)
     rows = activated.reshape(local_seqs * tokens, width)
-    glu_cols, out_cols = (
-        lax.all_gather(w_glu, "dp", axis=1, tiled=True),
-        lax.all_gather(w_out, "dp", axis=1, tiled=True),
-    )
+
+    def figure_match(patch):
+        return jnp.concatenate(lax.all_gather(patch, "dp"), 1)
+
+    glu_cols, out_cols = (figure_match(w_glu), lax.all_gather(w_out, "dp", axis=1, tiled=True))
     gate_pre = folder(rows, lax.all_gather(glu_cols, "sp", axis=0, tiled=True)) + b_glu
     gated = rows.astype(jnp.float32) * jax.nn.sigmoid(gate_pre)
     scale = lax.rsqrt(jnp.mean(gated * gated, axis=-1, keepdims=True) + 1e-06)

time: 148 us -> 149 us (level)
  waiting for transfers between devices: 17 us -> 20.3 us
  blocking collectives: 36.3 us -> 33.6 us
    all_gather x1, waiting for transfers between devices: 8.84 us -> 12.1 us  [per_device(): lax.all_gather(out_cols, 'sp', axis=0, tiled=True)]
    all_to_all x1, blocking collectives: 20.1 us -> 17.5 us  [per_device(): lax.all_to_all(local_act, 'sp', split_axis=1, concat_axis=2, tiled=True)]
    all_gather x1, blocking collectives: 7.76 us -> 6.26 us  [figure_match(): return jnp.concatenate(lax.all_gather(patch, 'dp'), 1)]
    unnamed x32 -> x35, local copies, waits for them, and re-layouts: 3.99 us -> 3.85 us
where the time goes in v1:
time: 149 us; the launch traced here: 148 us
  blocking collectives  33.6 us (23%)
  other arithmetic  33.5 us (22%)
  matrix products  30.4 us (20%)
  waiting for transfers between devices  20.3 us (14%)
  between operations  14.1 us (9%)
  local copies, waits for them, and re-layouts  10.5 us (7%)
  starting transfers between devices  5.99 us (4%)
    all_to_all x1, blocking collectives, per_device(): lax.all_to_all(local_act, 'sp', split_axis=1, concat_axis=2, tiled=True)  17.5 us
    sub x7, other arithmetic, mix_group(): inner_re + power_re * moved_re - power_im * moved_im  17.5 us
    unnamed x2, other arithmetic  13.8 us
    all_gather x1, waiting for transfers between devices, per_device(): lax.all_gather(out_cols, 'sp', axis=0, tiled=True)  12.1 us
    dot_general x1, matrix products, mix_group(): jnp.einsum('cp,kps->ksc', out_map[1], state_im, precision=highest)  11 us
    dot_general x1, matrix products, mix_group(): jnp.einsum('cp,kps->ksc', out_map[0], state_re, precision=highest)  9.95 us
    all_gather x1, blocking collectives, per_device(): lax.all_gather(w_out, 'dp', axis=1, tiled=True)  9.76 us
    all_to_all x1, waiting for transfers between devices, per_device(): lax.all_to_all(signal, 'sp', split_axis=2, concat_axis=1, tiled=True)  8.07 us
  transfers between devices with their start and end apart: 3, of which 2 were waited for; matrix products, arithmetic and copies ran while one was open for 46% of the time, Pallas kernels for 0%

profile of v1, /device:TPU:0, one launch (start us, length us, event | category | flops | bytes accessed | tf_op | source)
XLA Modules:
  0.0 148.2 jit_solution(15398461946471370925)
XLA Ops:
  6.5 6.3 %all-gather = bf16[128,512]{1,0:T(8,128)(2,1)S(1)} all-gather(bf16[64,512]{1,0:T(8,128)(2,1)} %param.26), channel_id=2, replica_groups=mesh['sp'=16,'dp'=2] {'dp'}, dimensions={0}, use_global_device_ids=true | all-gather | bytes 196608 | tf_op jit(solution)/shard_map/all_gather | solution.py:117
  12.9 0.7 copy.147
  13.7 9.8 %all_gather.18 = bf16[64,4096]{1,0:T(8,128)(2,1)} all-gather(bf16[64,2048]{1,0:T(8,128)(2,1)} %param.29), channel_id=1, replica_groups=mesh['sp'=16,'dp'=2] {'dp'}, dimensions={1}, use_global_device_ids=true | all-gather | bytes 786432 | tf_op jit(solution)/shard_map/all_gather | solution.py:119
  24.4 2.3 %reduce.14 = bf16[1024,128]{1,0:T(8,128)(2,1)S(1)} reduce(bf16[1024,1,128]{2,1,0:T(2,128)(2,1)S(1)} %bitcast.153, bf16[]{:T(256)} %broadcast.764), dimensions={1}, to_apply=%bitcast.96.reduce_sub_computation | reduce | bytes 524290
  26.7 0.8 reshape.461
  27.5 5.9 %all-to-all-start = ((bf16[16,2,4096]{2,1,0:T(2,128)(2,1)}), bf16[16,2,4096]{2,1,0:T(2,128)(2,1)S(1)}, u32[]{:S(2)}, u32[]{:S(2)}) async-start(bf16[16,2,4096]{2,1,0:T(2,128)(2,1)} %reshape.461), calls=%async_computation | async-start | bytes 524288 | tf_op jit(solution)/shard_map/all_to_all | solution.py:100
  35.5 8.1 %all-to-all-done = bf16[16,2,4096]{2,1,0:T(2,128)(2,1)S(1)} async-done(((bf16[16,2,4096]{2,1,0:T(2,128)(2,1)}), bf16[16,2,4096]{2,1,0:T(2,128)(2,1)S(1)}, u32[]{:S(2)}, u32[]{:S(2)}) %all-to-all-start) | async-done | bytes 262176 | tf_op jit(solution)/shard_map/all_to_all | solution.py:100
  44.2 1.4 fusion.48
  46.2 2.5 %fusion.4 = (f32[4,16,64,128]{3,2,1,0:T(8,128)S(1)}, f32[4,16,64,128]{3,2,1,0:T(8,128)S(1)}) fusion(f32[4,16,128,128]{3,2,1,0:T(8,128)S(1)} %fusion.48, f32[4,16,64,127]{3,2,1,0:T(8,128)S(1)} %get-tuple-element.102, f32[4,16,64,127]{3,2,1,0:T(8,128)S(1)} %get-tuple-element.101, f32[4,16,64]{2,1,0:T(8,128)S(1)} %get-tuple-element.151, ...), kind=kLoop, calls=%fused_computation.11 | loop fusion | flops 4194304 | bytes 12582912 | tf_op jit(solution)/shard_map/while/body/eval_jaxpr/vmap()/sub | solution.py:44
  48.7 2.5 %multiply_subtract_fusion.5 = (f32[4,16,64,128]{3,2,1,0:T(8,128)S(1)}, f32[4,16,64,128]{3,2,1,0:T(8,128)S(1)}) fusion(f32[4,16,64,128]{3,2,1,0:T(8,128)S(1)} %get-tuple-element.87, f32[4,16,64,126]{3,2,1,0:T(8,128)S(1)} %bitcast.139, f32[4,16,64,126]{3,2,1,0:T(8,128)S(1)} %bitcast.138, f32[4,16,64]{2,1,0:T(8,128)S(1)} %get-tuple-element.152, ...), kind=kLoop, calls=%fused_computation.34 | loop fusion | flops 4194304 | bytes 12550144 | tf_op jit(solution)/shard_map/while/body/eval_jaxpr/vmap()/sub | solution.py:44
  51.2 2.5 %multiply_subtract_fusion.4 = (f32[4,16,64,128]{3,2,1,0:T(8,128)S(1)}, f32[4,16,64,128]{3,2,1,0:T(8,128)S(1)}) fusion(f32[4,16,64,128]{3,2,1,0:T(8,128)S(1)} %get-tuple-element.99, f32[4,16,64,124]{3,2,1,0:T(8,128)S(1)} %bitcast.143, f32[4,16,64,124]{3,2,1,0:T(8,128)S(1)} %bitcast.142, f32[4,16,64]{2,1,0:T(8,128)S(1)} %get-tuple-element.148, ...), kind=kLoop, calls=%fused_computation.32 | loop fusion | flops 4194304 | bytes 12484608 | tf_op jit(solution)/shard_map/while/body/eval_jaxpr/vmap()/sub | solution.py:44
  53.7 2.5 %multiply_subtract_fusion.3 = (f32[4,16,64,128]{3,2,1,0:T(8,128)S(1)}, f32[4,16,64,128]{3,2,1,0:T(8,128)S(1)}) fusion(f32[4,16,64,128]{3,2,1,0:T(8,128)S(1)} %get-tuple-element.97, f32[4,16,64,120]{3,2,1,0:T(8,128)S(1)} %bitcast.145, f32[4,16,64,120]{3,2,1,0:T(8,128)S(1)} %bitcast.144, f32[4,16,64]{2,1,0:T(8,128)S(1)} %get-tuple-element.146, ...), kind=kLoop, calls=%fused_computation.30 | loop fusion | flops 4194304 | bytes 12353536 | tf_op jit(solution)/shard_map/while/body/eval_jaxpr/vmap()/sub | solution.py:44
  56.2 2.5 %multiply_subtract_fusion.2 = (f32[4,16,64,128]{3,2,1,0:T(8,128)S(1)}, f32[4,16,64,128]{3,2,1,0:T(8,128)S(1)}) fusion(f32[4,16,64,128]{3,2,1,0:T(8,128)S(1)} %get-tuple-element.95, f32[4,16,64,112]{3,2,1,0:T(8,128)S(1)} %bitcast.147, f32[4,16,64,112]{3,2,1,0:T(8,128)S(1)} %bitcast.146, f32[4,16,64]{2,1,0:T(8,128)S(1)} %get-tuple-element.144, ...), kind=kLoop, calls=%fused_computation.28 | loop fusion | flops 4194304 | bytes 12091392 | tf_op jit(solution)/shard_map/while/body/eval_jaxpr/vmap()/sub | solution.py:44
  58.7 2.5 %multiply_subtract_fusion.1 = (f32[4,16,64,128]{3,2,1,0:T(8,128)S(1)}, f32[4,16,64,128]{3,2,1,0:T(8,128)S(1)}) fusion(f32[4,16,64,128]{3,2,1,0:T(8,128)S(1)} %get-tuple-element.93, f32[4,16,64,96]{3,2,1,0:T(8,128)S(1)} %bitcast.149, f32[4,16,64,96]{3,2,1,0:T(8,128)S(1)} %bitcast.148, f32[4,16,64]{2,1,0:T(8,128)S(1)} %get-tuple-element.142, ...), kind=kLoop, calls=%fused_computation.26 | loop fusion | flops 4194304 | bytes 11567104 | tf_op jit(solution)/shard_map/while/body/eval_jaxpr/vmap()/sub | solution.py:44
  61.2 2.5 %multiply_subtract_fusion = (f32[4,16,64,128]{3,2,1,0:T(8,128)S(1)}, f32[4,16,64,128]{3,2,1,0:T(8,128)S(1)}) fusion(f32[4,16,64,128]{3,2,1,0:T(8,128)S(1)} %get-tuple-element.91, f32[4,16,64,64]{3,2,1,0:T(8,128)S(1)} %bitcast.141, f32[4,16,64,64]{3,2,1,0:T(8,128)S(1)} %bitcast.140, f32[4,16,64]{2,1,0:T(8,128)S(1)} %get-tuple-element.140, ...), kind=kLoop, calls=%fused_computation.24 | loop fusion | flops 4194304 | bytes 10518528 | tf_op jit(solution)/shard_map/while/body/eval_jaxpr/vmap()/sub | solution.py:44
  64.1 2.2 %slice_reduce_fusion = (f32[4,16,64]{2,1,0:T(8,128)S(1)}, f32[4,16,64]{2,1,0:T(8,128)S(1)}) fusion(f32[4,16,64,128]{3,2,1,0:T(8,128)S(1)} %get-tuple-element.90, f32[4,16,64,128]{3,2,1,0:T(8,128)S(1)} %get-tuple-element.89), kind=kLoop, calls=%fused_computation.6 | loop fusion | bytes 65536 | tf_op jit(solution)/shard_map/while/body/eval_jaxpr/vmap()/slice | solution.py:53
  68.2 11.0 %fusion.5 = f32[4,16,128,16]{2,3,1,0:T(8,128)S(1)} fusion(f32[4,16,64,128]{3,2,1,0:T(8,128)} %copy-done, f32[4,16,64]{2,1,0:T(8,128)S(1)} %pad_maximum_fusion.1, f32[4,16,64]{2,1,0:T(8,128)S(1)} %pad_maximum_fusion, f32[4,64]{1,0:T(4,128)S(1)} %copy-done.4, f32[4,16,128]{2,1,0:T(8,128)S(1)} %broadcast_multiply_fusion.6, f32[4,64]{1,0:T(4,128)S(1)} %copy-done.5, ...), kind=kOutput, calls=%fused_computation.12 | convolution fusion | flops 104857600 | bytes 2756608 | tf_op jit(solution)/shard_map/while/body/eval_jaxpr/vmap(cp,kps->ksc)/dot_general | solution.py:69
  79.2 10.0 %fusion.22 = f32[4,16,2,8,128]{4,3,2,1,0:T(8,128)S(1)} fusion(f32[4,16,128,16]{2,3,1,0:T(8,128)S(1)} %fusion.5, f32[4,16,64,128]{3,2,1,0:T(8,128)S(1)} %get-tuple-element.89, f32[4,16,64]{2,1,0:T(8,128)S(1)} %pad_maximum_fusion.1, f32[4,16,64]{2,1,0:T(8,128)S(1)} %pad_maximum_fusion, f32[4,64]{1,0:T(4,128)S(1)} %copy-done.4, ...), kind=kOutput, calls=%fused_computation.36 | convolution fusion | flops 104988672 | bytes 3280896 | tf_op jit(solution)/shard_map/while/body/eval_jaxpr/vmap(cp,kps->ksc)/dot_general | solution.py:69
  89.5 0.7 copy.131
  90.2 11.5 %reduce.15 = bf16[2048,64]{1,0:T(8,128)(2,1)S(1)} reduce(bf16[2048,1,64]{2,1,0:T(2,128)(2,1)S(1)} %bitcast.151, bf16[]{:T(256)} %broadcast.764), dimensions={1}, to_apply=%bitcast.98.reduce_sub_computation | reduce | bytes 524290
  102.2 17.5 %all_to_all.30 = bf16[16,2,4096]{2,1,0:T(2,128)(2,1)S(1)} all-to-all(bf16[16,2,4096]{2,1,0:T(2,128)(2,1)S(1)} %reshape.463), channel_id=1, replica_groups=mesh['sp'=16,'dp'=2] {'sp'}, dimensions={0} | all-to-all | bytes 524288 | tf_op jit(solution)/shard_map/all_to_all | solution.py:113
  121.3 2.3 %multiply_reduce_fusion = (f32[128]{0:T(128)S(1)}, f32[128,1024]{1,0:T(8,128)S(1)}) fusion(f32[1024]{0:T(1024)S(1)} %copy-done.10, bf16[128,1024]{0,1:T(8,128)(2,1)S(1)} %bitcast.157, bf16[1024,1024]{1,0:T(8,128)(2,1)} %all-gather.4.cloned.1.call-done, bf16[128,1024]{1,0:T(8,128)(2,1)S(1)} %copy.134), kind=kOutput, calls=%fused_computation.64 | convolution fusion | flops 269483904 | bytes 3150336 | tf_op jit(solution)/shard_map/dot_general | solution.py:77
  123.6 12.1 %all-gather.6.cloned.1.call-done = bf16[1024,4096]{1,0:T(8,128)(2,1)} async-done(((bf16[64,4096]{1,0:T(8,128)(2,1)}), bf16[1024,4096]{1,0:T(8,128)(2,1)}) %all-gather.6.cloned.1.call-update) | async-done | bytes 8388624 | tf_op jit(solution)/shard_map/all_gather | solution.py:124
  135.7 5.7 %fusion = bf16[1,128,4096]{2,1,0:T(8,128)(2,1)} fusion(bf16[1024,4096]{1,0:T(8,128)(2,1)} %all-gather.6.cloned.1.call-done, f32[128,1024]{1,0:T(8,128)S(1)} %get-tuple-element.161, f32[1024]{0:T(1024)S(1)} %copy-done.2, f32[128]{0:T(128)S(1)} %add_rsqrt_fusion), kind=kOutput, calls=%fused_computation.1 | convolution fusion | flops 1074659328 | bytes 9966080 | tf_op jit(solution)/shard_map/dot_general | solution.py:77
  (144 shorter events, 8.3 us)
Async XLA Ops:
  6.5 16.9 %copy-start.1 = (bf16[1,128,1024]{2,1,0:T(8,128)(2,1)S(1)}, bf16[1,128,1024]{2,1,0:T(8,128)(2,1)}, u32[]{:S(2)}) copy-start(bf16[1,128,1024]{2,1,0:T(8,128)(2,1)} %param.17) | copy-start | bytes 786436
  6.5 114.7 %all-gather.4.cloned.1.call-start = ((), (), s32[]{:S(2)}) async-start(), calls=%async_computation.2 | async-start | bytes 2228224 | tf_op jit(solution)/shard_map/all_gather | solution.py:120
  13.6 19.9 %copy-start.11 = (f32[4]{0:T(128)S(1)}, f32[4]{0:T(128)}, u32[]{:S(2)}) copy-start(f32[4]{0:T(128)} %param.19) | copy-start | bytes 52
  13.6 19.9 %copy-start.8 = (f32[1,16]{1,0:T(1,128)S(1)}, f32[1,16]{1,0:T(1,128)}, u32[]{:S(2)}) copy-start(f32[1,16]{1,0:T(1,128)} %param.18) | copy-start | bytes 196
  13.6 20.0 %copy-start.5 = (f32[4,64]{1,0:T(4,128)S(1)}, f32[4,64]{1,0:T(4,128)}, u32[]{:S(2)}) copy-start(f32[4,64]{1,0:T(4,128)} %param.20) | copy-start | bytes 3076
  13.6 20.1 %copy-start.4 = (f32[4,64]{1,0:T(4,128)S(1)}, f32[4,64]{1,0:T(4,128)}, u32[]{:S(2)}) copy-start(f32[4,64]{1,0:T(4,128)} %param.21) | copy-start | bytes 3076
  13.6 122.1 %all-gather.6.cloned.1.call-start = ((), (), s32[]{:S(2)}) async-start(), calls=%async_computation.3 | async-start | bytes 8912896 | tf_op jit(solution)/shard_map/all_gather | solution.py:124
  23.9 11.2 %copy-start.6 = (f32[1,2,4,64]{3,2,1,0:T(4,128)S(1)}, f32[1,2,4,64]{3,2,1,0:T(4,128)}, u32[]{:S(2)}) copy-start(f32[1,2,4,64]{3,2,1,0:T(4,128)} %param.25) | copy-start | bytes 6148
  24.4 10.8 %copy-start.7 = (f32[64]{0:T(128)S(1)}, f32[64]{0:T(128)}, u32[]{:S(2)}) copy-start(f32[64]{0:T(128)} %param.24) | copy-start | bytes 772
  24.4 10.9 %copy-start.3 = (f32[4,2,64,16]{2,3,1,0:T(8,128)S(1)}, f32[4,2,64,16]{2,3,1,0:T(8,128)}, u32[]{:S(2)}) copy-start(f32[4,2,64,16]{2,3,1,0:T(8,128)} %param.22) | copy-start | bytes 98308
  27.5 16.0 %all-to-all-start = ((bf16[16,2,4096]{2,1,0:T(2,128)(2,1)}), bf16[16,2,4096]{2,1,0:T(2,128)(2,1)S(1)}, u32[]{:S(2)}, u32[]{:S(2)}) async-start(bf16[16,2,4096]{2,1,0:T(2,128)(2,1)} %reshape.461), calls=%async_computation | async-start | bytes 524288 | tf_op jit(solution)/shard_map/all_to_all | solution.py:100
  63.8 2.6 %copy-start = (f32[4,16,64,128]{3,2,1,0:T(8,128)}, f32[4,16,64,128]{3,2,1,0:T(8,128)S(1)}, u32[]{:S(2)}) copy-start(f32[4,16,64,128]{3,2,1,0:T(8,128)S(1)} %get-tuple-element.90) | copy-start | bytes 6291460
  66.3 1.8 %copy-start.9 = (f32[4,2,16,64]{3,2,1,0:T(8,128)S(1)}, f32[4,2,16,64]{3,2,1,0:T(8,128)}, u32[]{:S(2)}) copy-start(f32[4,2,16,64]{3,2,1,0:T(8,128)} %param.23) | copy-start | bytes 98308
  119.7 1.6 %copy-start.10 = (f32[1024]{0:T(1024)S(1)}, f32[1024]{0:T(1024)}, u32[]{:S(2)}) copy-start(f32[1024]{0:T(1024)} %param.27) | copy-start | bytes 12292
  121.2 14.5 %copy-start.2 = (f32[1024]{0:T(1024)S(1)}, f32[1024]{0:T(1024)}, u32[]{:S(2)}) copy-start(f32[1024]{0:T(1024)} %param.28) | copy-start | bytes 12292
Sparse Core Ops, SparseCore 0:
  13.8 43.1 all-gather.3
  59.1 76.5 all-gather.5
